TPU v7x, 32 devices: a whole 2x2x4 slice. The times are simulated.
32 devices in a mesh: grp: 2 (over x), ep: 16 (over z, y, core).
Axes of the slice: x: 2, y: 2, z: 4, core: 2. Of those that a mesh axis runs over, the one named last changes fastest.
Arguments:
- tokens: bfloat16 [1024, 2048], P(('grp', 'ep')), parts along dimension 0, may hold values from -6 to 6
- routes: int32 [1024, 8], P(('grp', 'ep')), parts along dimension 0, may hold values from 0 to 15, all different within a row; in each aligned block of 32 rows (0 to 31, 32 to 63, ...) at most 24 rows name the same one
- gates: float32 [1024, 8], P(('grp', 'ep')), parts along dimension 0, may hold values from 0.1 to 0.6
- norm_gain: float32 [2048], replicated, may hold values from 0.1 to 1.9
- expert_gate: bfloat16 [16, 2048, 512], P('ep'), may hold values from -0.125 to 0.125
- expert_up: bfloat16 [16, 2048, 512], P('ep'), may hold values from -0.125 to 0.125
- expert_down: bfloat16 [16, 512, 2048], P('ep'), may hold values from -0.25 to 0.25
- shared_gate: bfloat16 [2048, 512], replicated, may hold values from -0.125 to 0.125
- shared_up: bfloat16 [2048, 512], replicated, may hold values from -0.125 to 0.125
- shared_down: bfloat16 [512, 2048], replicated, may hold values from -0.25 to 0.25
Outputs:
- mixed: bfloat16 [1024, 2048], P(('grp', 'ep')), parts along dimension 0
There are 2 independent parts, one for each index of `grp`. A program takes and returns all parts, laid end to end along the dimension named above; an argument that names none is the same for every part. Nothing has to cross between parts.
Inputs may be any that keep to these rules, and one draw needn't show every extreme that they name: `routes`: each row names 8 different experts; among the rows of one device no expert is named by more than 24 rows, a bound that some block reaches.
All inputs are finite; a program needn't handle non-finite values.
Results may differ from a plain program's by a relative error of at most 0.013.
Values may be sent and summed in bfloat16 or wider, within the bound.
No kernel may reach another device: no remote copies, remote signals or barrier semaphores. Data moves between devices by JAX's collectives and lax.ppermute only.
A program may use at most 128 MiB of HBM per device.

v0:
```python
import jax
import jax.numpy as jnp
from jax import lax
from jax.sharding import PartitionSpec as P


def norm_rows(tokens, norm_gain):
    values = tokens.astype(jnp.float32)
    scale = lax.rsqrt(jnp.mean(values * values, axis=-1, keepdims=True) + 1e-06)
    return (values * scale * norm_gain).astype(jnp.bfloat16)


def expert_rows(in_rows, w_gate, w_up, w_down):
    gate_pre = jnp.dot(in_rows, w_gate, preferred_element_type=jnp.float32)
    up_pre = jnp.dot(in_rows, w_up, preferred_element_type=jnp.float32)
    hidden = (jax.nn.silu(gate_pre) * up_pre).astype(jnp.bfloat16)
    return jnp.dot(hidden, w_down, preferred_element_type=jnp.float32).astype(jnp.bfloat16)


def slot_table(marks, capacity):
    before = jnp.cumsum(marks, axis=1) - marks
    slot_ids = jnp.arange(capacity, dtype=jnp.int32)
    picked = marks[:, None, :] * (before[:, None, :] == slot_ids[None, :, None]).astype(jnp.int32)
    places = jnp.arange(marks.shape[1], dtype=jnp.int32)
    return (jnp.sum(picked * places[None, None, :], axis=2), jnp.sum(picked, axis=2), before)


def shared_terms(normed, shared_gate, shared_up, shared_down):
    gate_pre = jnp.dot(normed, shared_gate, preferred_element_type=jnp.float32)
    up_pre = jnp.dot(normed, shared_up, preferred_element_type=jnp.float32)
    shared_hidden = (jax.nn.silu(gate_pre) * up_pre).astype(jnp.bfloat16)
    return jnp.dot(shared_hidden, shared_down, preferred_element_type=jnp.float32)


def local(
    tokens,
    routes,
    gates,
    norm_gain,
    expert_gate,
    expert_up,
    expert_down,
    shared_gate,
    shared_up,
    shared_down,
):
    rows_dev = tokens.shape[0]
    width = tokens.shape[1]
    groups = lax.axis_size("ep")
    capacity = 3 * rows_dev // 4
    normed = norm_rows(tokens, norm_gain)
    w_gate = expert_gate[0]
    w_up = expert_up[0]
    w_down = expert_down[0]
    shared = shared_terms(normed, shared_gate, shared_up, shared_down)
    naming = (routes[:, :, None] == jnp.arange(groups, dtype=jnp.int32)[None, None, :]).astype(
        jnp.int32
    )
    marks = jnp.sum(naming, axis=1).T
    slot_rows, filled, before = slot_table(marks, capacity)
    outbox = jnp.take(normed, slot_rows, axis=0)
    arrived = lax.all_to_all(outbox, "ep", split_axis=0, concat_axis=0, tiled=True)
    flat = arrived.reshape(-1, width)
    answers = expert_rows(flat, w_gate, w_up, w_down).reshape(arrived.shape)
    returned_rows = lax.all_to_all(answers, "ep", split_axis=0, concat_axis=0, tiled=True)
    slot_of = jnp.take_along_axis(before.T, routes, axis=1)
    fetched = returned_rows[routes, slot_of]
    routed = jnp.sum(gates[:, :, None] * fetched.astype(jnp.float32), axis=1)
    return (routed + shared).astype(jnp.bfloat16)


def solution(mesh):
    return jax.shard_map(
        local,
        mesh=mesh,
        in_specs=(
            P(("grp", "ep"), None),
            P(("grp", "ep"), None),
            P(("grp", "ep"), None),
            P(),
            P("ep", None, None),
            P("ep", None, None),
            P("ep", None, None),
            P(),
            P(),
            P(),
        ),
        out_specs=P(("grp", "ep"), None),
        check_vma=False,
    )
```

profile of v0, /device:TPU:15, one launch (start us, length us, event | category | flops | bytes accessed | tf_op | source)
XLA Modules:
  0.0 109.3 jit_solution(3239889930745548268)
XLA Ops:
  0.0 0.0 copy-start
  0.0 0.9 convert_reduce_fusion
  0.9 0.2 reduce_window_sum.13
  1.1 0.3 multiply_reduce_fusion
  1.4 0.1 reshape.52
  1.5 1.0 fusion.22
  2.6 1.0 fusion.24
  3.6 3.1 %gather_fusion = bf16[384,2048]{1,0:T(8,128)(2,1)} fusion(bf16[32,2048]{1,0:T(8,128)(2,1)S(1)} %fusion.24, s32[1024]{0:T(1024)S(1)} %pad_clamp_fusion), kind=kCustom, calls=%fused_computation | custom fusion | bytes 3147264 | tf_op jit(solution)/shard_map/jit(_take)/gather | solution.py:61
  6.7 1.6 %broadcast_select_fusion = bf16[16,24,2048]{2,1,0:T(8,128)(2,1)S(1)} fusion(bf16[16,24,2048]{2,1,0:T(8,128)(2,1)} %bitcast.40, pred[16,24]{1,0:T(8,128)(4,1)S(1)} %compare_and_fusion), kind=kLoop, calls=%fused_computation.13 | loop fusion | flops 786432 | bytes 3146112 | tf_op jit(solution)/shard_map/jit(_take)/select_n | solution.py:61
  8.3 0.0 copy-start.4
  8.4 42.5 %all_to_all.10 = bf16[16,24,2048]{2,1,0:T(8,128)(2,1)S(1)} all-to-all(bf16[16,24,2048]{2,1,0:T(8,128)(2,1)S(1)} %broadcast_select_fusion), channel_id=1, replica_groups=mesh['grp'=2,'ep'=16] {'ep'}, dimensions={0} | all-to-all | bytes 3145728 | tf_op jit(solution)/shard_map/all_to_all | solution.py:62
  50.9 0.0 copy-start.1
  50.9 1.1 %copy-done.1 = bf16[16,24,2048]{2,1,0:T(8,128)(2,1)} copy-done((bf16[16,24,2048]{2,1,0:T(8,128)(2,1)}, bf16[16,24,2048]{2,1,0:T(8,128)(2,1)S(1)}, u32[]{:S(2)}) %copy-start.1) | copy-done | bytes 1572888
  52.0 0.0 copy-done.4
  52.0 1.0 fusion.5
  53.0 0.0 copy-done
  53.0 5.1 %convolution_convert_fusion = bf16[384,2048]{1,0:T(8,128)(2,1)} fusion(bf16[1,512,2048]{2,1,0:T(8,128)(2,1)S(1)} %copy-done, bf16[384,2048]{1,0:T(8,128)(2,1)} %bitcast.43, bf16[1,2048,512]{2,1,0:T(8,128)(2,1)} %param.15, f32[384,512]{1,0:T(8,128)S(1)} %fusion.5), kind=kOutput, calls=%fused_computation.3 | convolution fusion | flops 1612578816 | bytes 8126464 | tf_op jit(solution)/shard_map/dot_general | solution.py:17
  58.1 0.0 copy-start.2
  58.1 5.1 %all-to-all-start.1 = ((bf16[16,24,2048]{2,1,0:T(8,128)(2,1)}), bf16[16,24,2048]{2,1,0:T(8,128)(2,1)}, u32[]{:S(2)}, u32[]{:S(2)}) async-start(bf16[16,24,2048]{2,1,0:T(8,128)(2,1)} %bitcast.41), calls=%async_computation.1 | async-start | bytes 3145728 | tf_op jit(solution)/shard_map/all_to_all | solution.py:65
  63.2 0.0 copy-done.2
  63.2 0.1 copy.19
  63.3 0.1 reshape.64
  63.4 0.0 copy-start.3
  63.4 2.0 %gather_fusion.2 = s32[256]{0:T(256)S(1)} fusion(s32[32,16]{0,1:T(8,128)S(1)} %bitcast_subtract_fusion, s32[256]{0:T(256)S(1)} %reshape.64), kind=kCustom, calls=%fused_computation.2 | custom fusion | bytes 4096 | tf_op jit(solution)/shard_map/jit(take_along_axis)/gather | solution.py:66
  65.5 0.1 reshape.67
  65.6 0.1 reshape.58
  65.7 0.0 copy-done.3
  65.7 0.7 copy.18
  66.3 2.7 %fusion.36 = f32[32,512]{1,0:T(8,128)} fusion(bf16[32,2048]{1,0:T(8,128)(2,1)S(1)} %fusion.24, bf16[2048,512]{1,0:T(8,128)(2,1)} %param.17), kind=kOutput, calls=%fused_computation.54 | convolution fusion | flops 67108864 | bytes 2293760 | tf_op jit(solution)/shard_map/dot_general | solution.py:29
  69.0 30.5 %all-to-all-done.1 = bf16[16,24,2048]{2,1,0:T(8,128)(2,1)} async-done(((bf16[16,24,2048]{2,1,0:T(8,128)(2,1)}), bf16[16,24,2048]{2,1,0:T(8,128)(2,1)}, u32[]{:S(2)}, u32[]{:S(2)}) %all-to-all-start.1) | async-done | bytes 1572896 | tf_op jit(solution)/shard_map/all_to_all | solution.py:65
  99.5 4.3 %gather_fusion.1 = bf16[256,2048]{1,0:T(8,128)(2,1)S(1)} fusion(bf16[16,24,2048]{2,1,0:T(8,128)(2,1)} %all-to-all-done.1, s32[256]{0:T(256)S(1)} %reshape.58), kind=kCustom, calls=%fused_computation.1 | custom fusion | bytes 2099200 | tf_op jit(solution)/shard_map/gather | solution.py:67
  103.8 1.7 %fusion.1 = f32[32,2048]{1,0:T(8,128)S(1)} fusion(bf16[256,2048]{1,0:T(8,128)(2,1)S(1)} %gather_fusion.1, f32[32,8]{1,0:T(8,128)} %copy.18), kind=kLoop, calls=%fused_computation.7 | loop fusion | flops 1507328 | bytes 1311744 | tf_op jit(solution)/shard_map/reduce_sum | solution.py:68
  105.5 3.8 %fusion = bf16[32,2048]{1,0:T(8,128)(2,1)} fusion(f32[32,2048]{1,0:T(8,128)S(1)} %fusion.1, bf16[512,2048]{1,0:T(8,128)(2,1)} %param.19, bf16[32,2048]{1,0:T(8,128)(2,1)S(1)} %fusion.24, bf16[2048,512]{1,0:T(8,128)(2,1)} %param.18, f32[32,512]{1,0:T(8,128)} %fusion.36), kind=kOutput, calls=%fused_computation.5 | convolution fusion | flops 134447104 | bytes 4784128 | tf_op jit(solution)/shard_map/dot_general | solution.py:32
  (8 shorter events, 0.1 us)
Async XLA Ops:
  0.0 53.0 %copy-start = (bf16[1,512,2048]{2,1,0:T(8,128)(2,1)S(1)}, bf16[1,512,2048]{2,1,0:T(8,128)(2,1)}, u32[]{:S(2)}) copy-start(bf16[1,512,2048]{2,1,0:T(8,128)(2,1)} %param.16) | copy-start | bytes 6291460
  8.3 43.7 %copy-start.4 = (bf16[1,2048,512]{2,1,0:T(8,128)(2,1)S(1)}, bf16[1,2048,512]{2,1,0:T(8,128)(2,1)}, u32[]{:S(2)}) copy-start(bf16[1,2048,512]{2,1,0:T(8,128)(2,1)} %param.14) | copy-start | bytes 6291460
  50.9 1.1 %copy-start.1 = (bf16[16,24,2048]{2,1,0:T(8,128)(2,1)}, bf16[16,24,2048]{2,1,0:T(8,128)(2,1)S(1)}, u32[]{:S(2)}) copy-start(bf16[16,24,2048]{2,1,0:T(8,128)(2,1)S(1)} %all_to_all.10) | copy-start | bytes 4718596
  58.1 5.1 %copy-start.2 = (s32[32,8]{0,1:T(8,128)S(1)}, s32[32,8]{0,1:T(8,128)}, u32[]{:S(2)}) copy-start(s32[32,8]{0,1:T(8,128)} %param.11) | copy-start | bytes 3076
  58.1 41.4 %all-to-all-start.1 = ((bf16[16,24,2048]{2,1,0:T(8,128)(2,1)}), bf16[16,24,2048]{2,1,0:T(8,128)(2,1)}, u32[]{:S(2)}, u32[]{:S(2)}) async-start(bf16[16,24,2048]{2,1,0:T(8,128)(2,1)} %bitcast.41), calls=%async_computation.1 | async-start | bytes 3145728 | tf_op jit(solution)/shard_map/all_to_all | solution.py:65
  63.4 2.2 %copy-start.3 = (f32[32,8]{0,1:T(8,128)S(1)}, f32[32,8]{0,1:T(8,128)}, u32[]{:S(2)}) copy-start(f32[32,8]{0,1:T(8,128)} %param.12) | copy-start | bytes 3076
where the time goes:
time: 110 us; the launch traced here: 109 us
  blocking collectives  42.5 us (39%)
  waiting for transfers between devices  30.5 us (28%)
  matrix products  12.6 us (11%)
  local copies, waits for them, and re-layouts  11.7 us (11%)
  other arithmetic  6.83 us (6%)
  starting transfers between devices  5.09 us (5%)
    all_to_all x1, blocking collectives, local(): lax.all_to_all(outbox, 'ep', split_axis=0, concat_axis=0, tiled=True)  42.5 us
    all_to_all x1, waiting for transfers between devices, local(): lax.all_to_all(answers, 'ep', split_axis=0, concat_axis=0, tiled=True)  30.5 us
    dot_general x1, matrix products, expert_rows(): jnp.dot(hidden, w_down, preferred_element_type=jnp.float32)  5.15 us
    all_to_all x1, starting transfers between devices, local(): lax.all_to_all(answers, 'ep', split_axis=0, concat_axis=0, tiled=True)  5.09 us
    gather x1, local copies, waits for them, and re-layouts, local(): fetched = returned_rows[routes, slot_of]  4.26 us
    dot_general x1, matrix products, shared_terms(): jnp.dot(shared_hidden, shared_down, preferred_element_type=jnp.float32)  3.83 us
    gather x1, local copies, waits for them, and re-layouts, local(): outbox = jnp.take(normed, slot_rows, axis=0)  3.13 us
    dot_general x1, matrix products, shared_terms(): gate_pre = jnp.dot(normed, shared_gate, preferred_element_type=jnp.float32)  2.67 us
  transfers between devices with their start and end apart: 1, of which 1 were waited for; matrix products, arithmetic and copies ran while one was open for 5% of the time, Pallas kernels for 0%

commit v1 on v0

v1 whole, which is shorter than its diff:
```python
import jax
import jax.numpy as jnp
from jax import lax
from jax.sharding import PartitionSpec as P


def norm_rows(tokens, norm_gain):
    values = tokens.astype(jnp.float32)
    scale = lax.rsqrt(jnp.mean(values * values, axis=-1, keepdims=True) + 1e-06)
    return (values * scale * norm_gain).astype(jnp.bfloat16)


def ffn(in_rows, w_gate, w_up, w_down):
    gate_pre = jnp.dot(in_rows, w_gate, preferred_element_type=jnp.float32)
    up_pre = jnp.dot(in_rows, w_up, preferred_element_type=jnp.float32)
    hidden = (jax.nn.silu(gate_pre) * up_pre).astype(jnp.bfloat16)
    return jnp.dot(hidden, w_down, preferred_element_type=jnp.float32)


def split3(x):
    a = lax.reduce_precision(x, 8, 7)
    b = lax.reduce_precision(x - a, 8, 7)
    c = x - a - b
    return [v.astype(jnp.bfloat16) for v in (a, b, c)]


def local(
    tokens, routes, gates, norm_gain,
    expert_gate, expert_up, expert_down,
    shared_gate, shared_up, shared_down,
):
    width = tokens.shape[1]
    groups = lax.axis_size("ep")
    me = lax.axis_index("ep")
    normed = norm_rows(tokens, norm_gain)
    naming = routes[:, :, None] == jnp.arange(groups, dtype=jnp.int32)[None, None, :]
    weights = jnp.sum(jnp.where(naming, gates[:, :, None], 0.0), axis=1)
    cols = jnp.concatenate(split3(weights), axis=1)
    pad = -cols.shape[1] % 128
    cols = jnp.pad(cols, ((0, 0), (0, pad)))
    sent = jnp.concatenate([normed, cols], axis=1)
    every = lax.all_gather(sent, "ep", axis=0, tiled=True)
    shared = ffn(normed, shared_gate, shared_up, shared_down)
    flat = every[:, :width]
    lane = jnp.arange(groups * 3, dtype=jnp.int32) % groups
    extra = every[:, width : width + 3 * groups].astype(jnp.float32)
    mine = jnp.sum(jnp.where(lane[None, :] == me, extra, 0.0), axis=1, keepdims=True)
    answers = ffn(flat, expert_gate[0], expert_up[0], expert_down[0])
    partial = (mine * answers.astype(jnp.bfloat16).astype(jnp.float32)).astype(jnp.bfloat16)
    routed = lax.psum_scatter(partial, "ep", scatter_dimension=0, tiled=True)
    return (routed.astype(jnp.float32) + shared).astype(jnp.bfloat16)


def solution(mesh):
    return jax.shard_map(
        local,
        mesh=mesh,
        in_specs=(
            P(("grp", "ep"), None),
            P(("grp", "ep"), None),
            P(("grp", "ep"), None),
            P(),
            P("ep", None, None),
            P("ep", None, None),
            P("ep", None, None),
            P(),
            P(),
            P(),
        ),
        out_specs=P(("grp", "ep"), None),
        check_vma=False,
    )
```

time: 110 us -> 137 us (1.25)
  the two profiles are of different devices: /device:TPU:15 before, /device:TPU:0 now
where the time goes in v1:
time: 137 us
  waiting for transfers between devices  103 us (75%)
  matrix products  15.3 us (11%)
  between operations  13.4 us (10%)
  other arithmetic  4.66 us (3%)
    reduce_scatter x1, waiting for transfers between devices, local(): routed = lax.psum_scatter(partial, 'ep', scatter_dimension=0, tiled=True)  58.4 us
    all_gather x1, waiting for transfers between devices, local(): every = lax.all_gather(sent, 'ep', axis=0, tiled=True)  44.7 us
    dot_general x2, matrix products, ffn(): return jnp.dot(hidden, w_down, preferred_element_type=jnp.float32)  9.8 us
    dot_general x2, matrix products, ffn(): gate_pre = jnp.dot(in_rows, w_gate, preferred_element_type=jnp.float32)  5.51 us
  transfers between devices with their start and end apart: 2, of which 2 were waited for; matrix products, arithmetic and copies ran while one was open for 1% of the time, Pallas kernels for 0%

profile of v1, /device:TPU:0, one launch (start us, length us, event | category | flops | bytes accessed | tf_op | source)
XLA Modules:
  0.0 136.7 jit_solution(5991184890525336149)
XLA Ops:
  6.5 0.0 copy-start
  6.5 0.0 all-gather.2.cloned.1.call-start
  6.5 0.9 select_reduce_fusion.1
  7.4 0.1 copy.14
  7.5 1.0 fusion.25
  8.6 1.0 fusion.27
  9.6 0.7 fusion.28
  10.3 0.0 all-gather.2.cloned.1.call-update
  10.3 0.0 reduce-scatter.2.cloned.1.call-start
  10.4 44.7 %all-gather.2.cloned.1.call-done = bf16[512,2176]{1,0:T(8,128)(2,1)} async-done(((bf16[32,2176]{1,0:T(8,128)(2,1)}), bf16[512,2176]{1,0:T(8,128)(2,1)}) %all-gather.2.cloned.1.call-update) | async-done | bytes 2228240 | tf_op jit(solution)/shard_map/all_gather | solution.py:42
  55.1 3.5 %fusion.4 = f32[512,512]{1,0:T(8,128)S(1)} fusion(bf16[1,2048,512]{2,1,0:T(8,128)(2,1)} %param.14, bf16[512,2176]{1,0:T(8,128)(2,1)} %all-gather.2.cloned.1.call-done), kind=kOutput, calls=%fused_computation.7 | convolution fusion | flops 1073741824 | bytes 5242880 | tf_op jit(solution)/shard_map/dot_general | solution.py:14
  58.6 1.0 select_reduce_fusion
  59.6 0.0 copy-done
  59.6 6.0 %multiply_convert_fusion = bf16[512,2048]{1,0:T(8,128)(2,1)} fusion(bf16[1,512,2048]{2,1,0:T(8,128)(2,1)S(1)} %copy-done, f32[512]{0:T(512)S(1)} %select_reduce_fusion, bf16[1,2048,512]{2,1,0:T(8,128)(2,1)} %param.15, bf16[512,2176]{1,0:T(8,128)(2,1)} %all-gather.2.cloned.1.call-done, f32[512,512]{1,0:T(8,128)S(1)} %fusion.4), kind=kOutput, calls=%fused_computation | convolution fusion | flops 2153250816 | bytes 9439232 | tf_op jit(solution)/shard_map/dot_general | solution.py:17
  65.6 0.0 reduce-scatter.2.cloned.1.call-update
  65.7 2.0 %fusion.39 = f32[32,512]{1,0:T(8,128)S(1)} fusion(bf16[32,2048]{1,0:T(8,128)(2,1)S(1)} %fusion.27, bf16[2048,512]{1,0:T(8,128)(2,1)} %param.17), kind=kOutput, calls=%fused_computation.44 | convolution fusion | flops 67108864 | bytes 2293760 | tf_op jit(solution)/shard_map/dot_general | solution.py:14
  67.7 58.4 %reduce-scatter.2.cloned.1.call-done = bf16[32,2048]{1,0:T(8,128)(2,1)} async-done(((bf16[512,2048]{1,0:T(8,128)(2,1)}), bf16[32,2048]{1,0:T(8,128)(2,1)}) %reduce-scatter.2.cloned.1.call-update) | async-done | bytes 131088 | tf_op jit(solution)/shard_map/reduce_scatter | solution.py:50
  126.1 3.8 %fusion = bf16[32,2048]{1,0:T(8,128)(2,1)} fusion(bf16[512,2048]{1,0:T(8,128)(2,1)} %param.19, bf16[32,2048]{1,0:T(8,128)(2,1)S(1)} %fusion.27, bf16[2048,512]{1,0:T(8,128)(2,1)} %param.18, bf16[32,2048]{1,0:T(8,128)(2,1)} %reduce-scatter.2.cloned.1.call-done, f32[32,512]{1,0:T(8,128)S(1)} %fusion.39), kind=kOutput, calls=%fused_computation.3 | convolution fusion | flops 134512640 | bytes 4653056 | tf_op jit(solution)/shard_map/dot_general | solution.py:17
  (4 shorter events, 0.0 us)
Async XLA Ops:
  6.5 53.1 %copy-start = (bf16[1,512,2048]{2,1,0:T(8,128)(2,1)S(1)}, bf16[1,512,2048]{2,1,0:T(8,128)(2,1)}, u32[]{:S(2)}) copy-start(bf16[1,512,2048]{2,1,0:T(8,128)(2,1)} %param.16) | copy-start | bytes 6291460
  6.5 48.6 %all-gather.2.cloned.1.call-start = ((), (), s32[]{:S(2)}) async-start(), calls=%async_computation.1 | async-start | bytes 2367488 | tf_op jit(solution)/shard_map/all_gather | solution.py:42
  10.3 115.8 %reduce-scatter.2.cloned.1.call-start = ((), (), s32[]{:S(2)}) async-start(), calls=%async_computation.2 | async-start | bytes 2228224 | tf_op jit(solution)/shard_map/reduce_scatter | solution.py:50
Sparse Core Ops, SparseCore 0:
  10.4 44.6 all-gather.1
  65.8 60.2 reduce-scatter.1
